TPU v7x, 32 devices: a whole 2x2x4 slice. The times are simulated.
32 devices in a mesh: kv: 16 (over z, y, x), tp: 2 (over core).
Axes of the slice: x: 2, y: 2, z: 4, core: 2. Of those that a mesh axis runs over, the one named last changes fastest.
Arguments:
- tokens: bfloat16 [32, 4096], P(None, 'kv'), may hold values from -16 to 16
- mix_gain: bfloat16 [4096], P('kv'), may hold values from 0.099609375 to 1.8984375
- ffn_gain: bfloat16 [4096], P('kv'), may hold values from 0.099609375 to 1.8984375
- w_query: bfloat16 [4096, 2048], P('kv', 'tp'), may hold values from -0.09375 to 0.09375
- w_key: bfloat16 [4096, 2048], P('kv', 'tp'), may hold values from -0.09375 to 0.09375
- w_value: bfloat16 [4096, 4096], P('kv', 'tp'), may hold values from -0.09375 to 0.09375
- w_gate: bfloat16 [4096, 4096], P('kv', 'tp'), may hold values from -0.09375 to 0.09375
- w_decay: bfloat16 [4096, 2048], P('kv', 'tp'), may hold values from -0.375 to 0.375
- decay_bias: float32 [2048], P('tp'), may hold values from -7 to 4
- head_gain: bfloat16 [512], replicated, may hold values from 0.099609375 to 1.8984375
- w_output: bfloat16 [4096, 4096], P('tp', 'kv'), may hold values from -0.09375 to 0.09375
- w_ffgate: bfloat16 [4096, 11008], P('kv', 'tp'), may hold values from -0.09375 to 0.09375
- w_ffup: bfloat16 [4096, 11008], P('kv', 'tp'), may hold values from -0.09375 to 0.09375
- w_down: bfloat16 [11008, 4096], P('tp', 'kv'), may hold values from -0.0546875 to 0.0546875
- state: float32 [32, 8, 256, 512], P('kv', 'tp'), may hold values from -6 to 6
Outputs:
- mixed: bfloat16 [32, 4096], P(None, 'kv')
- new_state: float32 [32, 8, 256, 512], P('kv', 'tp')
All inputs are finite; a program needn't handle non-finite values.
Results may differ from a plain program's by a relative error of at most 0.015.
Values may be sent and summed in bfloat16 or wider, within the bound.
No kernel may reach another device: no remote copies, remote signals or barrier semaphores. Data moves between devices by JAX's collectives and lax.ppermute only.
A program may use at most 64 MiB of HBM per device.

v0:
```python
import jax
import jax.numpy as jnp
from jax import lax
from jax.sharding import PartitionSpec as P

epsilon = 1e-06


def local(
    tokens,
    mix_gain,
    ffn_gain,
    w_query,
    w_key,
    w_value,
    w_gate,
    w_decay,
    decay_bias,
    head_gain,
    w_output,
    w_ffgate,
    w_ffup,
    w_down,
    state,
):
    own_rows = state.shape[0]
    local_heads = state.shape[1]
    key_dim = state.shape[2]
    val_dim = state.shape[3]
    model_width = tokens.shape[1] * lax.axis_size("kv")
    row_offset = lax.axis_index("kv") * own_rows
    token_f32 = tokens.astype(jnp.float32)
    row_squares = jnp.sum(token_f32 * token_f32, axis=1)
    mix_in = (token_f32 * mix_gain.astype(jnp.float32)).astype(jnp.bfloat16)
    query_part = jnp.dot(mix_in, w_query, preferred_element_type=jnp.float32)
    key_part = jnp.dot(mix_in, w_key, preferred_element_type=jnp.float32)
    value_part = jnp.dot(mix_in, w_value, preferred_element_type=jnp.float32)
    gate_part = jnp.dot(mix_in, w_gate, preferred_element_type=jnp.float32)
    decay_part = jnp.dot(mix_in, w_decay, preferred_element_type=jnp.float32)
    square_total = lax.psum(row_squares, "kv")
    own_squares = lax.dynamic_slice_in_dim(square_total, row_offset, own_rows)
    query_sum, key_sum, value_sum, gate_sum, decay_sum = (
        lax.psum_scatter(query_part, "kv", scatter_dimension=0, tiled=True),
        lax.psum_scatter(key_part, "kv", scatter_dimension=0, tiled=True),
        lax.psum_scatter(value_part, "kv", scatter_dimension=0, tiled=True),
        lax.psum_scatter(gate_part, "kv", scatter_dimension=0, tiled=True),
        lax.psum_scatter(decay_part, "kv", scatter_dimension=0, tiled=True),
    )
    mix_rms = lax.rsqrt(own_squares / model_width + epsilon)[:, None]
    queries = (query_sum * mix_rms).reshape(own_rows, local_heads, key_dim) * key_dim ** (-0.5)
    key_rows = (key_sum * mix_rms).reshape(own_rows, local_heads, key_dim)
    value_rows = (value_sum * mix_rms).reshape(own_rows, local_heads, val_dim)
    gate_rows = (gate_sum * mix_rms).reshape(own_rows, local_heads, val_dim)
    decay_rows = (decay_sum * mix_rms + decay_bias).reshape(own_rows, local_heads, key_dim)
    log_decay = jax.nn.log_sigmoid(decay_rows) / 16.0
    new_state = (
        jnp.exp(log_decay)[..., None] * state + key_rows[..., :, None] * value_rows[..., None, :]
    )
    attended = jnp.einsum("bhk,bhkv->bhv", queries, new_state, precision=lax.Precision.HIGHEST)
    attended = attended * lax.rsqrt(
        jnp.sum(attended * attended, axis=2, keepdims=True) / val_dim + epsilon
    )
    head_out = (
        (attended * head_gain.astype(jnp.float32) * jax.nn.silu(gate_rows))
        .reshape(own_rows, local_heads * val_dim)
        .astype(jnp.bfloat16)
    )
    head_partial = jnp.dot(
        lax.all_gather(head_out, "kv", axis=0, tiled=True),
        w_output,
        preferred_element_type=jnp.float32,
    )
    attn_out = lax.psum(head_partial.astype(jnp.bfloat16), "tp").astype(jnp.float32)
    residual_mid = (token_f32 + attn_out).astype(jnp.bfloat16)
    mid_f32 = residual_mid.astype(jnp.float32)
    mid_squares = jnp.sum(mid_f32 * mid_f32, axis=1)
    ffn_in = (mid_f32 * ffn_gain.astype(jnp.float32)).astype(jnp.bfloat16)
    ffgate_part = jnp.dot(ffn_in, w_ffgate, preferred_element_type=jnp.float32)
    ffup_part = jnp.dot(ffn_in, w_ffup, preferred_element_type=jnp.float32)
    ffgate_sum, ffup_sum, square_sum = lax.psum((ffgate_part, ffup_part, mid_squares), "kv")
    ffn_rms = lax.rsqrt(square_sum / model_width + epsilon)[:, None]
    hidden = (jax.nn.silu(ffgate_sum * ffn_rms) * (ffup_sum * ffn_rms)).astype(jnp.bfloat16)
    down_part = jnp.dot(hidden, w_down, preferred_element_type=jnp.float32)
    ffn_out = lax.psum(down_part.astype(jnp.bfloat16), "tp").astype(jnp.float32)
    mixed = (mid_f32 + ffn_out).astype(jnp.bfloat16)
    return (mixed, new_state)


def solution(mesh):
    in_specs = (
        P(None, "kv"),
        P("kv"),
        P("kv"),
        P("kv", "tp"),
        P("kv", "tp"),
        P("kv", "tp"),
        P("kv", "tp"),
        P("kv", "tp"),
        P("tp"),
        P(),
        P("tp", "kv"),
        P("kv", "tp"),
        P("kv", "tp"),
        P("tp", "kv"),
        P("kv", "tp", None, None),
    )
    out_specs = (P(None, "kv"), P("kv", "tp", None, None))
    return jax.shard_map(local, mesh=mesh, in_specs=in_specs, out_specs=out_specs, check_vma=False)
```

profile of v0, /device:TPU:0, one launch (start us, length us, event | category | flops | bytes accessed | tf_op | source)
XLA Modules:
  0.0 317.6 jit_solution(6141432531111428591)
XLA Ops:
  7.2 0.0 copy-start
  7.2 0.0 copy-start.7
  7.2 0.0 copy-start.3
  7.2 0.0 copy-start.6
  7.2 0.0 copy-start.5
  7.2 0.0 copy-start.4
  7.2 0.0 all-reduce.12.cloned.1.call-start
  7.3 0.8 convert_element_type.49
  8.1 1.9 fusion.28
  10.0 1.9 fusion.26
  11.9 1.9 fusion.30
  13.9 2.2 fusion.24
  16.1 2.2 fusion.22
  18.3 0.0 all-reduce.12.cloned.1.call-update
  18.3 0.0 all-reduce.10.cloned.1.call-start
  18.4 0.0 copy-done.6
  18.4 0.0 copy-done.5
  18.5 0.0 copy-done.7
  18.5 0.6 dynamic-slice
  19.7 0.0 copy-done.3
  19.7 0.1 fusion.3
  19.8 43.7 %psum.42 = f32[32]{0:T(128)S(1)} all-reduce(f32[32]{0:T(128)S(1)} %fusion.3), channel_id=1, replica_groups=mesh['kv'=16,'tp'=2] {'kv'}, use_global_device_ids=true, to_apply=%region_2.0 | all-reduce | flops 32 | bytes 256 | tf_op jit(solution)/shard_map/psum | solution.py:40
  63.6 0.1 add_rsqrt_fusion.2
  63.6 70.8 %all-reduce.12.cloned.1.call-done = (f32[32,2048]{1,0:T(8,128)}, f32[32,1024]{1,0:T(8,128)}, f32[32,2048]{1,0:T(8,128)}, f32[32,1024]{1,0:T(8,128)}, f32[32,1024]{1,0:T(8,128)}) async-done(((f32[32,2048]{1,0:T(8,128)}, f32[32,1024]{1,0:T(8,128)}, f32[32,2048]{1,0:T(8,128)}, f32[32,1024]{1,0:T(8,128)}, f32[32,1024]{1,0:T(8,128)}), (f32[32,2048]{1,0:T(8,128)}, f32[32,1024]{1,0:T(8,128)}, ...) | async-done | bytes 917520
  134.4 0.0 copy-done.4
  134.4 0.9 fusion.20
  135.4 1.0 dynamic-slice_multiply_fusion.1
  136.4 2.6 multiply_add_fusion
  139.0 0.0 copy-start.1
  139.0 2.0 copy-done.1
  141.0 2.1 fusion.34
  143.1 0.1 fusion.9
  143.2 0.1 fusion.11
  143.3 39.5 %all-gather = bf16[16,2,2048]{2,1,0:T(2,128)(2,1)S(1)} all-gather(bf16[1,2,2048]{2,1,0:T(2,128)(2,1)S(1)} %reshape.47), channel_id=1, replica_groups=mesh['kv'=16,'tp'=2] {'kv'}, dimensions={0}, use_global_device_ids=true | all-gather | bytes 139264 | tf_op jit(solution)/shard_map/all_gather | solution.py:69
  182.9 0.1 reshape.48
  182.9 1.5 convolution_convert_fusion.1
  184.4 3.4 %psum.43 = bf16[32,256]{1,0:T(8,128)(2,1)S(1)} all-reduce(bf16[32,256]{1,0:T(8,128)(2,1)S(1)} %convolution_convert_fusion.1), channel_id=1, replica_groups=mesh['kv'=16,'tp'=2] {'tp'}, use_global_device_ids=true, to_apply=%region_8.9 | all-reduce | flops 8192 | bytes 32768 | tf_op jit(solution)/shard_map/psum | solution.py:73
  187.8 0.0 copy-start.2
  187.8 0.1 fusion.6
  187.9 0.0 copy-done
  187.9 1.5 fusion.12
  189.4 0.5 copy-done.2
  189.8 1.4 fusion.14
  191.3 0.0 all-reduce.10.cloned.1.call-update
  191.3 36.9 %psum.45 = f32[32]{0:T(128)S(1)} all-reduce(f32[32]{0:T(128)S(1)} %get-tuple-element.9), channel_id=1, replica_groups=mesh['kv'=16,'tp'=2] {'kv'}, use_global_device_ids=true, to_apply=%region_11.12 | all-reduce | flops 32 | bytes 256 | tf_op jit(solution)/shard_map/psum | solution.py:80
  228.2 75.7 %all-reduce.10.cloned.1.call-done = (f32[32,5504]{1,0:T(8,128)}, f32[32,5504]{1,0:T(8,128)}) async-done(((f32[32,5504]{1,0:T(8,128)}, f32[32,5504]{1,0:T(8,128)}), (f32[32,5504]{1,0:T(8,128)}, f32[32,5504]{1,0:T(8,128)})) %all-reduce.10.cloned.1.call-update) | async-done | bytes 1409040 | tf_op jit(solution)/shard_map/psum | solution.py:80
  303.9 2.8 convolution_convert_fusion
  306.8 3.4 %psum.47 = bf16[32,256]{1,0:T(8,128)(2,1)S(1)} all-reduce(bf16[32,256]{1,0:T(8,128)(2,1)S(1)} %convolution_convert_fusion), channel_id=1, replica_groups=mesh['kv'=16,'tp'=2] {'tp'}, use_global_device_ids=true, to_apply=%region_13.14 | all-reduce | flops 8192 | bytes 32768 | tf_op jit(solution)/shard_map/psum | solution.py:84
  310.1 0.6 fusion.7
  (11 shorter events, 0.2 us)
Async XLA Ops:
  7.2 180.7 %copy-start = (bf16[256,5504]{1,0:T(8,128)(2,1)S(1)}, bf16[256,5504]{1,0:T(8,128)(2,1)}, u32[]{:S(2)}) copy-start(bf16[256,5504]{1,0:T(8,128)(2,1)} %param.27) | copy-start | bytes 8454148
  7.2 11.3 %copy-start.7 = (u32[32]{0:T(128)S(1)}, u32[32]{0:T(128)}, u32[]{:S(2)}) copy-start(u32[32]{0:T(128)} %constant.41) | copy-start | bytes 388
  7.2 12.5 %copy-start.3 = (bf16[32,256]{1,0:T(8,128)(2,1)S(1)}, bf16[32,256]{1,0:T(8,128)(2,1)}, u32[]{:S(2)}) copy-start(bf16[32,256]{1,0:T(8,128)(2,1)} %param.15) | copy-start | bytes 49156
  7.2 11.2 %copy-start.6 = (bf16[256]{0:T(256)(128)(2,1)S(1)}, bf16[256]{0:T(256)(128)(2,1)}, u32[]{:S(2)}) copy-start(bf16[256]{0:T(256)(128)(2,1)} %param.17) | copy-start | bytes 1540
  7.2 11.2 %copy-start.5 = (bf16[512]{0:T(512)(128)(2,1)S(1)}, bf16[512]{0:T(512)(128)(2,1)}, u32[]{:S(2)}) copy-start(bf16[512]{0:T(512)(128)(2,1)} %param.24) | copy-start | bytes 3076
  7.2 127.2 %copy-start.4 = (f32[1024]{0:T(1024)S(1)}, f32[1024]{0:T(1024)}, u32[]{:S(2)}) copy-start(f32[1024]{0:T(1024)} %param.23) | copy-start | bytes 12292
  7.2 127.2 %all-reduce.12.cloned.1.call-start = ((), (), s32[]{:S(2)}) async-start(), calls=%async_computation.1 | async-start | bytes 1835008
  18.3 285.6 %all-reduce.10.cloned.1.call-start = ((), (), s32[]{:S(2)}) async-start(), calls=%async_computation | async-start | bytes 2818048 | tf_op jit(solution)/shard_map/psum | solution.py:80
  139.0 2.0 copy-start.1
  187.8 2.1 copy-start.2
Sparse Core Ops, SparseCore 0:
  18.5 115.9 all-reduce.11
  191.4 112.4 all-reduce.9
where the time goes:
time: 318 us
  waiting for transfers between devices  147 us (46%)
  blocking collectives  127 us (40%)
  matrix products  19.6 us (6%)
  between operations  14.9 us (5%)
  other arithmetic  6.37 us (2%)
  local copies, waits for them, and re-layouts  3.25 us (1%)
    psum x1, waiting for transfers between devices, local(): lax.psum((ffgate_part, ffup_part, mid_squares), 'kv')  75.7 us
    unnamed x3, waiting for transfers between devices  70.8 us
    psum x1, blocking collectives, local(): square_total = lax.psum(row_squares, 'kv')  43.7 us
    all_gather x1, blocking collectives, local(): lax.all_gather(head_out, 'kv', axis=0, tiled=True)  39.5 us
    psum x1, blocking collectives, local(): lax.psum((ffgate_part, ffup_part, mid_squares), 'kv')  36.9 us
  transfers between devices with their start and end apart: 2, of which 2 were waited for; matrix products, arithmetic and copies ran while one was open for 0% of the time, Pallas kernels for 0%

commit v1 on v0

v1 whole, which is shorter than its diff:
```python
import functools

import jax
import jax.numpy as jnp
from jax import lax
from jax.experimental import pallas as pl
from jax.experimental.pallas import tpu as pltpu
from jax.sharding import PartitionSpec as P


epsilon = 1e-06
f32 = jnp.float32
bf16 = jnp.bfloat16
LANES = 128
VMEM = pl.BlockSpec(memory_space=pltpu.VMEM)
HBM = pl.BlockSpec(memory_space=pltpu.HBM)


def exchange(value, axis, size, mask):
    return lax.ppermute(value, axis, [(i, i ^ mask) for i in range(size)])


def padded(width):
    return -(-width // LANES) * LANES


def call(body, outs, operands, flops, read, scratch=(), specs=None, vmem=16 << 20, out_specs=None):
    if specs:
        operands = [pltpu.with_memory_space_constraint(x, pltpu.HBM) if spec is HBM else x for x, spec in zip(operands, specs)]
    return pl.pallas_call(
        body,
        out_shape=[jax.ShapeDtypeStruct(shape, dtype) for shape, dtype in outs],
        in_specs=specs or [VMEM] * len(operands),
        out_specs=out_specs or [VMEM] * len(outs),
        scratch_shapes=list(scratch),
        cost_estimate=pl.CostEstimate(flops=flops, bytes_accessed=read, transcendentals=0),
        compiler_params=pltpu.CompilerParams(vmem_limit_bytes=vmem),
    )(*operands)


def store_squares(values, parts, at):
    sums = jnp.sum(values * values, axis=1, keepdims=True)
    high = sums.astype(bf16).astype(f32)
    lane = lax.broadcasted_iota(jnp.int32, (values.shape[0], LANES), 1)
    tail = jnp.where(lane == 0, high, jnp.where(lane == 1, sums - high, 0.0)).astype(bf16)
    rows = parts[0].shape[0]
    for s, part in enumerate(parts):
        part[:, at:at + LANES] = tail[s * rows:(s + 1) * rows]


def store_product(left, weight, parts, at, step=512):
    rows = parts[0].shape[0]
    width = weight.shape[1]
    for low in range(0, width, step):
        high = min(width, low + step)
        product = jnp.dot(left, weight[:, low:high], preferred_element_type=f32).astype(bf16)
        for s, part in enumerate(parts):
            part[:, at + low:at + high] = product[s * rows:(s + 1) * rows]
    if padded(width) > width:
        for part in parts:
            part[:, at + width:at + padded(width)] = jnp.zeros((rows, padded(width) - width), bf16)


def project_kernel(inner, perm, *refs):
    sources, refs = refs[:7], refs[7:]
    ordered, parts, refs = refs[0], refs[1:1 + inner], refs[1 + inner:]
    held, sems = refs[:7], refs[7]
    copies = [pltpu.make_async_copy(w, h, sems.at[i]) for i, (w, h) in enumerate(zip(sources, held))]
    for copy in copies:
        copy.start()
    copies[0].wait()
    copies[1].wait()
    token_f32 = jnp.dot(perm[...], held[0][...], preferred_element_type=f32)
    ordered[...] = token_f32.astype(bf16)
    mix_in = (token_f32 * held[1][...].astype(f32).reshape(1, -1)).astype(bf16)
    at = 0
    store_squares(token_f32, parts, sum(padded(w.shape[1]) for w in held[2:]))
    for copy, h in zip(copies[2:], held[2:]):
        copy.wait()
        store_product(mix_in, h, parts, at)
        at += padded(h.shape[1])


def attend_kernel(own, heads, key_dim, val_dim, width, bias, gain, state, *refs):
    pieces, (out, turned, values, rows, flat) = refs[:-5], refs[-5:]
    total = pieces[0][...].astype(f32)
    for piece in pieces[1:]:
        total = total + piece[...].astype(f32)
    keys, vals = heads * key_dim, heads * val_dim
    at_key, at_value = padded(keys), 2 * padded(keys)
    at_gate = at_value + padded(vals)
    at_decay = at_gate + padded(vals)
    at_squares = at_decay + padded(keys)
    squares = total[:, at_squares:at_squares + 1] + total[:, at_squares + 1:at_squares + 2]
    rms = lax.rsqrt(squares / width + epsilon)
    query = total[:, :keys] * rms * key_dim ** (-0.5)
    key = total[:, at_key:at_key + keys] * rms
    value = total[:, at_value:at_value + vals] * rms
    gate = total[:, at_gate:at_gate + vals] * rms
    pre = total[:, at_decay:at_decay + keys] * rms + bias[...]
    log_decay = -(jnp.maximum(-pre, 0.0) + jnp.log1p(jnp.exp(-jnp.abs(pre)))) / 16.0
    decay = jnp.exp(log_decay)
    scaled = query * decay
    gated = gate / (1.0 + jnp.exp(-gate))
    product = query * key
    count = own * heads
    rows[...] = jnp.zeros_like(rows)
    for b in range(own):
        for h in range(heads):
            i = b * heads + h
            cut = slice(h * key_dim, (h + 1) * key_dim)
            rows[i:i + 1, :] = scaled[b:b + 1, cut]
            rows[count + i:count + i + 1, :] = decay[b:b + 1, cut]
            rows[2 * count + i:2 * count + i + 1, :] = key[b:b + 1, cut]
            values[i:i + 1, :] = value[b:b + 1, h * val_dim:(h + 1) * val_dim]
    columns = jnp.transpose(rows[...])
    turned[...] = columns
    for b in range(own):
        for h in range(heads):
            i = b * heads + h
            cut = slice(h * val_dim, (h + 1) * val_dim)
            dot = jnp.sum(product[b:b + 1, h * key_dim:(h + 1) * key_dim], axis=1, keepdims=True)
            attended = jnp.sum(columns[:, i:i + 1] * state[b, h], axis=0, keepdims=True) + dot * value[b:b + 1, cut]
            scale = lax.rsqrt(jnp.sum(attended * attended, axis=1, keepdims=True) / val_dim + epsilon)
            flat[b:b + 1, cut] = attended * scale * gain[...].astype(f32) * gated[b:b + 1, cut]
    out[...] = flat[...].astype(bf16)


def fetch_kernel(state, weight, state_out, weight_out, sems):
    count, depth = state.shape[0], weight.shape[0] // 2
    copies = [pltpu.make_async_copy(state.at[b, h], state_out.at[b, h], sems.at[b * state.shape[1] + h])
              for b in range(count) for h in range(state.shape[1])]
    last = len(copies)
    copies += [pltpu.make_async_copy(weight.at[pl.ds(i * depth, depth)], weight_out.at[pl.ds(i * depth, depth)], sems.at[last + i])
               for i in range(2)]
    for copy in copies:
        copy.start()
    for copy in copies:
        copy.wait()


def state_kernel(own, heads, turned, values, state, new_state, held, sems):
    count = own * heads
    copies = []
    for b in range(own):
        for h in range(heads):
            i = b * heads + h
            decay = turned[:, count + i:count + i + 1]
            key = turned[:, 2 * count + i:2 * count + i + 1]
            held[b, h] = decay * state[b, h] + key * values[i:i + 1, :]
            copies.append(pltpu.make_async_copy(held.at[b, h], new_state.at[b, h], sems.at[i]))
            copies[-1].start()
    for copy in copies:
        copy.wait()


def multiply_kernel(weight, *refs):
    left, out = refs[:-1], refs[-1]
    rows = jnp.concatenate([ref[...] for ref in left], axis=0)
    out[...] = jnp.dot(rows, weight[...], preferred_element_type=f32).astype(bf16)


def ffn_kernel(groups, tokens, gain, gate, up, *refs):
    partials, middle, parts = refs[:groups], refs[groups], refs[groups + 1:]
    total = partials[0][...].astype(f32)
    for partial in partials[1:]:
        total = total + partial[...].astype(f32)
    middle[...] = (tokens[...].astype(f32) + total).astype(bf16)
    mid = middle[...].astype(f32)
    ffn_in = (mid * gain[...].astype(f32)).astype(bf16)
    units = padded(gate.shape[1])
    store_squares(mid, parts, 2 * units)
    store_product(ffn_in, gate, parts, 0)
    store_product(ffn_in, up, parts, units)


def hidden_kernel(units, width, *refs):
    pieces, out = refs[:-1], refs[-1]
    total = pieces[0][...].astype(f32)
    for piece in pieces[1:]:
        total = total + piece[...].astype(f32)
    at = padded(units)
    squares = total[:, 2 * at:2 * at + 1] + total[:, 2 * at + 1:2 * at + 2]
    rms = lax.rsqrt(squares / width + epsilon)
    gate = total[:, :units] * rms
    out[...] = (gate / (1.0 + jnp.exp(-gate)) * (total[:, at:at + units] * rms)).astype(bf16)


def final_kernel(perm, middle, *refs):
    partials, out = refs[:-1], refs[-1]
    total = partials[0][...].astype(f32)
    for partial in partials[1:]:
        total = total + partial[...].astype(f32)
    mixed = (middle[...].astype(f32) + total).astype(bf16)
    back = lax.dot_general(perm[...], mixed, (((0,), (0,)), ((), ())), preferred_element_type=f32)
    out[...] = back.astype(bf16)


def reduce_rows(parts, size, inner):
    outer = size // inner
    sent = [exchange(parts[s], "kv", size, s) for s in range(1, inner)]
    total = parts[0].astype(f32)
    for value in sent:
        total = total + value.astype(f32)
    blocks = total.astype(bf16).reshape(outer, total.shape[0] // outer, total.shape[1])
    return [blocks[0]] + [exchange(blocks[u], "kv", size, u * inner) for u in range(1, outer)]


def gather_rows(rows, size, inner):
    outer = size // inner
    sent = [exchange(rows, "kv", size, u * inner) for u in range(1, outer)]
    rows = jnp.concatenate([rows] + sent, 0)
    return [rows] + [exchange(rows, "kv", size, s) for s in range(1, inner)]


def over_tp(part, size):
    return [part] + [exchange(part, "tp", size, mask) for mask in range(1, size)]


def local(size, groups, inner, tokens, mix_gain, ffn_gain, w_query, w_key, w_value, w_gate, w_decay, decay_bias, head_gain,
          w_output, w_ffgate, w_ffup, w_down, state):
    own, heads, key_dim, val_dim = state.shape
    seqs, channels = tokens.shape
    width = channels * size
    outer = size // inner
    index = jnp.arange(seqs, dtype=jnp.int32)
    block = index // own
    source = ((block // outer + block % outer * inner) ^ lax.axis_index("kv")) * own + index % own
    perm = (source[:, None] == index[None, :]).astype(bf16)

    weights = (w_query, w_key, w_value, w_gate, w_decay)
    total = sum(padded(w.shape[1]) for w in weights) + LANES
    rows = seqs // inner
    ordered, *parts = call(
        functools.partial(project_kernel, inner),
        [((seqs, channels), bf16)] + [((rows, total), bf16)] * inner,
        (perm, tokens, mix_gain, *weights),
        2 * seqs * channels * total, 2 * channels * total,
        scratch=[pltpu.VMEM(w.shape, bf16) for w in (tokens, mix_gain, *weights)] + [pltpu.SemaphoreType.DMA((7,))],
        specs=[VMEM] + [HBM] * 7,
    )
    held_state, held_output = call(
        fetch_kernel, [(state.shape, f32), (w_output.shape, bf16)], (state, w_output),
        0, 4 * state.size + 2 * w_output.size,
        scratch=[pltpu.SemaphoreType.DMA((own * heads + 2,))], specs=[HBM] * 2, vmem=1 << 20,
    )
    pieces = reduce_rows(parts, size, inner)
    count = own * heads
    deep = -(-3 * count // 8) * 8
    head_out, turned, values = call(
        functools.partial(attend_kernel, own, heads, key_dim, val_dim, width),
        [((own, heads * val_dim), bf16), ((key_dim, deep), f32), ((count, val_dim), f32)],
        (decay_bias.reshape(1, -1), head_gain.reshape(1, -1), held_state, *pieces),
        4 * state.size, 4 * state.size,
        scratch=[pltpu.VMEM((deep, key_dim), f32), pltpu.VMEM((own, heads * val_dim), f32)],
    )
    new_state, = call(
        functools.partial(state_kernel, own, heads), [(state.shape, f32)], (turned, values, held_state),
        4 * state.size, 8 * state.size,
        scratch=[pltpu.VMEM(state.shape, f32), pltpu.SemaphoreType.DMA((count,))],
        out_specs=[HBM],
    )
    gathered = gather_rows(head_out, size, inner)
    partial, = call(multiply_kernel, [((seqs, channels), bf16)], (held_output, *gathered),
                    2 * seqs * w_output.size, 2 * w_output.size)
    units = w_ffgate.shape[1]
    middle, *parts = call(
        functools.partial(ffn_kernel, groups),
        [((seqs, channels), bf16)] + [((rows, 2 * padded(units) + LANES), bf16)] * inner,
        (ordered, ffn_gain.reshape(1, -1), w_ffgate, w_ffup, *over_tp(partial, groups)),
        4 * seqs * w_ffgate.size, 4 * w_ffgate.size,
    )
    pieces = reduce_rows(parts, size, inner)
    hidden, = call(functools.partial(hidden_kernel, units, width), [((own, units), bf16)], pieces,
                   32 * own * units, 8 * own * units)
    gathered = gather_rows(hidden, size, inner)
    partial, = call(multiply_kernel, [((seqs, channels), bf16)], (w_down, *gathered),
                    2 * seqs * w_down.size, 2 * w_down.size)
    mixed, = call(final_kernel, [((seqs, channels), bf16)], (perm, middle, *over_tp(partial, groups)),
                  4 * seqs * channels, 8 * seqs * channels)
    return (mixed, new_state)


def solution(mesh):
    size, groups = mesh.shape["kv"], mesh.shape["tp"]
    if size & (size - 1) or groups & (groups - 1):
        raise ValueError("axis sizes")
    inner = 1 << ((size.bit_length() - 1) // 2)
    rows, columns = P("tp", "kv"), P("kv", "tp")
    in_specs = (P(None, "kv"), P("kv"), P("kv"), columns, columns, columns, columns, columns, P("tp"), P(), rows, columns, columns,
                rows, P("kv", "tp", None, None))
    out_specs = (P(None, "kv"), P("kv", "tp", None, None))

    def body(*args):
        return local(size, groups, inner, *args)

    return jax.shard_map(body, mesh=mesh, in_specs=in_specs, out_specs=out_specs, check_vma=False)
```

time: 318 us -> 78.5 us (0.25)
  blocking collectives: 127 us -> 0 us
  waiting for transfers between devices: 147 us -> 32.3 us
  starting transfers between devices: 0.08 us -> 33.3 us
  matrix products: 19.6 us -> 0 us
  between operations: 14.9 us -> 0.82 us
  Pallas kernels: 0 us -> 11.3 us
  other arithmetic: 6.37 us -> 0.39 us
    psum x4 -> x0, blocking collectives: 87.3 us -> none  [the longest x1 43.7 us: local(): square_total = lax.psum(row_squares, 'kv')]
    psum x1 -> x0, waiting for transfers between devices: 75.7 us -> none  [local(): lax.psum((ffgate_part, ffup_part, mid_squares), 'kv')]
    unnamed x3 -> x0, waiting for transfers between devices: 70.8 us -> none
    all_gather x1 -> x0, blocking collectives: 39.5 us -> none  [local(): lax.all_gather(head_out, 'kv', axis=0, tiled=True)]
    ppermute x0 -> x26, starting transfers between devices: none -> 33.3 us  [exchange(): return lax.ppermute(value, axis, [(i, i ^ mask) for i in range(size)])]
    ppermute x0 -> x26, waiting for transfers between devices: none -> 32.3 us  [exchange(): return lax.ppermute(value, axis, [(i, i ^ mask) for i in range(size)])]
    dot_general x10 -> x0, matrix products: 19.6 us -> none  [the longest x1 2.84 us: local(): down_part = jnp.dot(hidden, w_down, preferred_element_type=jnp.float32)]
    pallas_call x0 -> x9, Pallas kernels: none -> 11.3 us  [call(): pl.pallas_call(body, out_shape=[jax.ShapeDtypeStruct(shape, dtype) for sh...]
  transfers between devices with their start and end apart: 2 -> 26, of which waited for: 2 -> 21; matrix products, arithmetic and copies ran while one was open for 0% -> 0% of each run, Pallas kernels for 0% -> 6%
where the time goes in v1:
time: 78.5 us; the launch traced here: 78.3 us
  starting transfers between devices  33.3 us (42%)
  waiting for transfers between devices  32.3 us (41%)
  Pallas kernels  11.3 us (14%)
  between operations  0.82 us (1%)
    ppermute x26, starting transfers between devices, exchange(): return lax.ppermute(value, axis, [(i, i ^ mask) for i in range(size)])  33.3 us
    ppermute x26, waiting for transfers between devices, exchange(): return lax.ppermute(value, axis, [(i, i ^ mask) for i in range(size)])  32.3 us
    pallas_call x9, Pallas kernels, call(): pl.pallas_call(body, out_shape=[jax.ShapeDtypeStruct(shape, dtype) for sh...  11.3 us
  transfers between devices with their start and end apart: 26, of which 21 were waited for; matrix products, arithmetic and copies ran while one was open for 0% of the time, Pallas kernels for 6%

profile of v1, /device:TPU:0, one launch (start us, length us, event | category | flops | bytes accessed | tf_op | source)
XLA Modules:
  0.0 78.3 jit_solution(17374992089058872746)
XLA Ops:
  0.7 0.1 fusion.perm
  0.7 2.5 %shard_map.158 = (bf16[32,256]{1,0:T(8,128)(2,1)S(1)}, bf16[8,7296]{1,0:T(8,128)(2,1)S(1)}, bf16[8,7296]{1,0:T(8,128)(2,1)S(1)}, bf16[8,7296]{1,0:T(8,128)(2,1)S(1)}, bf16[8,7296]{1,0:T(8,128)(2,1)S(1)}) custom-call(bf16[32,32]{1,0:T(8,128)(2,1)S(1)} %fusion.perm, bf16[32,256]{1,0:T(8,128)(2,1)} %refs_0_.1, bf16[256]{0:T(256)(128)(2,1)} %refs_1_.1, ...), custom_call_target="tpu_custom_call" | custom-call | flops 119537664 | bytes 3735552 | tf_op jit(solution)/shard_map/pallas_call | solution.py:30
  3.2 4.0 %collective-permute-start.2 = (bf16[8,7296]{1,0:T(8,128)(2,1)S(1)}, bf16[8,7296]{1,0:T(8,128)(2,1)S(1)}, u32[]{:S(2)}, u32[]{:S(2)}) collective-permute-start(bf16[8,7296]{1,0:T(8,128)(2,1)S(1)} %get-tuple-element.23), channel_id=1, source_target_pairs={{0,6},{2,4},{4,2},{6,0},{8,14},{10,12},{12,10},{14,8},{16,22},{18,... | collective-permute-start | bytes 350216 | tf_op jit(solution)/shard_map/ppermute | solution.py:20
  7.2 0.5 collective-permute-start.1
  7.7 0.1 collective-permute-start
  7.8 2.9 %collective-permute-done.2 = bf16[8,7296]{1,0:T(8,128)(2,1)S(1)} collective-permute-done((bf16[8,7296]{1,0:T(8,128)(2,1)S(1)}, bf16[8,7296]{1,0:T(8,128)(2,1)S(1)}, u32[]{:S(2)}, u32[]{:S(2)}) %collective-permute-start.2) | collective-permute-done | bytes 116768 | tf_op jit(solution)/shard_map/ppermute | solution.py:20
  10.8 2.1 %collective-permute-done.1 = bf16[8,7296]{1,0:T(8,128)(2,1)S(1)} collective-permute-done((bf16[8,7296]{1,0:T(8,128)(2,1)S(1)}, bf16[8,7296]{1,0:T(8,128)(2,1)S(1)}, u32[]{:S(2)}, u32[]{:S(2)}) %collective-permute-start.1) | collective-permute-done | bytes 116768 | tf_op jit(solution)/shard_map/ppermute | solution.py:20
  12.9 0.2 collective-permute-done
  13.1 0.1 add_convert_fusion.1
  13.2 0.1 fusion.5
  13.3 1.6 %collective-permute-start.3 = (bf16[2,7296]{1,0:T(2,128)(2,1)S(1)}, bf16[2,7296]{1,0:T(2,128)(2,1)S(1)}, u32[]{:S(2)}, u32[]{:S(2)}) collective-permute-start(bf16[2,7296]{1,0:T(2,128)(2,1)S(1)} %get-tuple-element.38), channel_id=1, source_target_pairs={{0,8},{2,10},{4,12},{6,14},{8,0},{10,2},{12,4},{14,6},{16,24},{18,... | collective-permute-start | bytes 87560 | tf_op jit(solution)/shard_map/ppermute | solution.py:20
  14.9 2.6 %collective-permute-start.4 = (bf16[2,7296]{1,0:T(2,128)(2,1)S(1)}, bf16[2,7296]{1,0:T(2,128)(2,1)S(1)}, u32[]{:S(2)}, u32[]{:S(2)}) collective-permute-start(bf16[2,7296]{1,0:T(2,128)(2,1)S(1)} %get-tuple-element.37), channel_id=1, source_target_pairs={{0,16},{2,18},{4,20},{6,22},{8,24},{10,26},{12,28},{14,30},{16,0},... | collective-permute-start | bytes 87560 | tf_op jit(solution)/shard_map/ppermute | solution.py:20
  17.5 0.2 collective-permute-start.5
  17.8 0.0 copy-start
  17.8 0.0 copy-start.1
  17.8 2.7 %shard_map.159 = (f32[2,4,256,512]{3,2,1,0:T(8,128)S(1)}, bf16[2048,256]{1,0:T(8,128)(2,1)S(1)}) custom-call(f32[2,4,256,512]{3,2,1,0:T(8,128)} %state.1, bf16[2048,256]{1,0:T(8,128)(2,1)} %weight.2), custom_call_target="tpu_custom_call" | custom-call | bytes 5242880 | tf_op jit(solution)/shard_map/pallas_call | solution.py:30
  20.5 0.0 collective-permute-done.3.refs_1_
  20.5 2.7 %collective-permute-done.5.refs_3_ = bf16[2,7296]{1,0:T(2,128)(2,1)S(1)} collective-permute-done((bf16[2,7296]{1,0:T(2,128)(2,1)S(1)}, bf16[2,7296]{1,0:T(2,128)(2,1)S(1)}, u32[]{:S(2)}, u32[]{:S(2)}) %collective-permute-start.5) | collective-permute-done | bytes 29216 | tf_op jit(solution)/shard_map/ppermute | solution.py:20
  23.2 1.1 %shard_map.160 = (bf16[2,2048]{1,0:T(2,128)(2,1)S(1)}, f32[256,24]{1,0:T(8,128)S(1)}, f32[8,512]{1,0:T(8,128)S(1)}) custom-call(f32[1,1024]{1,0:T(1,128)S(1)} %bitcast.1, bf16[1,512]{1,0:T(2,128)(2,1)S(1)} %reshape.84.gain, f32[2,4,256,512]{3,2,1,0:T(8,128)S(1)} %get-tuple-element.19.state, bf16[2,7296]{1,0:T(2,128)(2,1)S(1)} %get-tuple-element.39.refs_0_, ...), custom_call_target="tpu_custom_call" | custom-call | flops 4194304 | bytes 4194304 | tf_op jit(solution)/shard_map/pallas_call | solution.py:30
  24.3 1.0 %collective-permute-start.8 = (bf16[2,2048]{1,0:T(2,128)(2,1)S(1)}, bf16[2,2048]{1,0:T(2,128)(2,1)S(1)}, u32[]{:S(2)}, u32[]{:S(2)}) collective-permute-start(bf16[2,2048]{1,0:T(2,128)(2,1)S(1)} %get-tuple-element.24), channel_id=1, source_target_pairs={{0,24},{2,26},{4,28},{6,30},{8,16},{10,18},{12,20},{14,22},{16,8},... | collective-permute-start | bytes 24584 | tf_op jit(solution)/shard_map/ppermute | solution.py:20
  25.3 3.5 %collective-permute-start.6 = (bf16[2,2048]{1,0:T(2,128)(2,1)S(1)}, bf16[2,2048]{1,0:T(2,128)(2,1)S(1)}, u32[]{:S(2)}, u32[]{:S(2)}) collective-permute-start(bf16[2,2048]{1,0:T(2,128)(2,1)S(1)} %get-tuple-element.24), channel_id=1, source_target_pairs={{0,8},{2,10},{4,12},{6,14},{8,0},{10,2},{12,4},{14,6},{16,24},{18,... | collective-permute-start | bytes 24584 | tf_op jit(solution)/shard_map/ppermute | solution.py:20
  28.8 1.1 %collective-permute-done.8 = bf16[2,2048]{1,0:T(2,128)(2,1)S(1)} collective-permute-done((bf16[2,2048]{1,0:T(2,128)(2,1)S(1)}, bf16[2,2048]{1,0:T(2,128)(2,1)S(1)}, u32[]{:S(2)}, u32[]{:S(2)}) %collective-permute-start.8) | collective-permute-done | bytes 8224 | tf_op jit(solution)/shard_map/ppermute | solution.py:20
  29.8 0.2 collective-permute-done.7
  30.0 0.4 collective-permute-done.6
  30.5 1.6 %collective-permute-start.9 = (bf16[8,2048]{1,0:T(8,128)(2,1)S(1)}, bf16[8,2048]{1,0:T(8,128)(2,1)S(1)}, u32[]{:S(2)}, u32[]{:S(2)}) collective-permute-start(bf16[8,2048]{1,0:T(8,128)(2,1)S(1)} %pad_maximum_fusion.1.refs_0_), channel_id=1, source_target_pairs={{0,2},{2,0},{4,6},{6,4},{8,10},{10,8},{12,14},{14,12},{16,18},{18,... | collective-permute-start | bytes 98312 | tf_op jit(solution)/shard_map/ppermute | solution.py:20
  32.1 0.7 collective-permute-start.10
  32.8 1.2 %collective-permute-start.11 = (bf16[8,2048]{1,0:T(8,128)(2,1)S(1)}, bf16[8,2048]{1,0:T(8,128)(2,1)S(1)}, u32[]{:S(2)}, u32[]{:S(2)}) collective-permute-start(bf16[8,2048]{1,0:T(8,128)(2,1)S(1)} %pad_maximum_fusion.1.refs_0_), channel_id=1, source_target_pairs={{0,6},{2,4},{4,2},{6,0},{8,14},{10,12},{12,10},{14,8},{16,22},{18,... | collective-permute-start | bytes 98312 | tf_op jit(solution)/shard_map/ppermute | solution.py:20
  34.0 0.4 collective-permute-done.9.refs_1_
  34.4 1.5 %collective-permute-done.10.refs_2_ = bf16[8,2048]{1,0:T(8,128)(2,1)S(1)} collective-permute-done((bf16[8,2048]{1,0:T(8,128)(2,1)S(1)}, bf16[8,2048]{1,0:T(8,128)(2,1)S(1)}, u32[]{:S(2)}, u32[]{:S(2)}) %collective-permute-start.10) | collective-permute-done | bytes 32800 | tf_op jit(solution)/shard_map/ppermute | solution.py:20
  36.0 1.6 %collective-permute-done.11.refs_3_ = bf16[8,2048]{1,0:T(8,128)(2,1)S(1)} collective-permute-done((bf16[8,2048]{1,0:T(8,128)(2,1)S(1)}, bf16[8,2048]{1,0:T(8,128)(2,1)S(1)}, u32[]{:S(2)}, u32[]{:S(2)}) %collective-permute-start.11) | collective-permute-done | bytes 32800 | tf_op jit(solution)/shard_map/ppermute | solution.py:20
  37.6 0.3 shard_map.161.refs_0_
  37.9 0.0 collective-permute-start.12
  37.9 1.2 %collective-permute-done.12.refs_1_ = bf16[32,256]{1,0:T(8,128)(2,1)S(1)} collective-permute-done((bf16[32,256]{1,0:T(8,128)(2,1)S(1)}, bf16[32,256]{1,0:T(8,128)(2,1)S(1)}, u32[]{:S(2)}, u32[]{:S(2)}) %collective-permute-start.12) | collective-permute-done | bytes 16416 | tf_op jit(solution)/shard_map/ppermute | solution.py:20
  39.1 0.9 %shard_map.162 = (bf16[32,256]{1,0:T(8,128)(2,1)S(1)}, bf16[8,11136]{1,0:T(8,128)(2,1)S(1)}, bf16[8,11136]{1,0:T(8,128)(2,1)S(1)}, bf16[8,11136]{1,0:T(8,128)(2,1)S(1)}, bf16[8,11136]{1,0:T(8,128)(2,1)S(1)}) custom-call(bf16[32,256]{1,0:T(8,128)(2,1)S(1)} %get-tuple-element.17.tokens, bf16[1,256]{1,0:T(2,128)(2,1)S(1)} %reshape.82.gain, ...), custom_call_target="tpu_custom_call" | custom-call | flops 180355072 | bytes 5636096 | tf_op jit(solution)/shard_map/pallas_call | solution.py:30
  40.0 1.3 %collective-permute-start.15 = (bf16[8,11136]{1,0:T(8,128)(2,1)S(1)}, bf16[8,11136]{1,0:T(8,128)(2,1)S(1)}, u32[]{:S(2)}, u32[]{:S(2)}) collective-permute-start(bf16[8,11136]{1,0:T(8,128)(2,1)S(1)} %get-tuple-element.29), channel_id=1, source_target_pairs={{0,6},{2,4},{4,2},{6,0},{8,14},{10,12},{12,10},{14,8},{16,22},{18,... | collective-permute-start | bytes 534536 | tf_op jit(solution)/shard_map/ppermute | solution.py:20
  41.3 1.5 %collective-permute-start.14 = (bf16[8,11136]{1,0:T(8,128)(2,1)S(1)}, bf16[8,11136]{1,0:T(8,128)(2,1)S(1)}, u32[]{:S(2)}, u32[]{:S(2)}) collective-permute-start(bf16[8,11136]{1,0:T(8,128)(2,1)S(1)} %get-tuple-element.28), channel_id=1, source_target_pairs={{0,4},{2,6},{4,0},{6,2},{8,12},{10,14},{12,8},{14,10},{16,20},{18,... | collective-permute-start | bytes 534536 | tf_op jit(solution)/shard_map/ppermute | solution.py:20
  42.8 0.8 %collective-permute-start.13 = (bf16[8,11136]{1,0:T(8,128)(2,1)S(1)}, bf16[8,11136]{1,0:T(8,128)(2,1)S(1)}, u32[]{:S(2)}, u32[]{:S(2)}) collective-permute-start(bf16[8,11136]{1,0:T(8,128)(2,1)S(1)} %get-tuple-element.27), channel_id=1, source_target_pairs={{0,2},{2,0},{4,6},{6,4},{8,10},{10,8},{12,14},{14,12},{16,18},{18,... | collective-permute-start | bytes 534536 | tf_op jit(solution)/shard_map/ppermute | solution.py:20
  43.6 4.8 %collective-permute-done.15 = bf16[8,11136]{1,0:T(8,128)(2,1)S(1)} collective-permute-done((bf16[8,11136]{1,0:T(8,128)(2,1)S(1)}, bf16[8,11136]{1,0:T(8,128)(2,1)S(1)}, u32[]{:S(2)}, u32[]{:S(2)}) %collective-permute-start.15) | collective-permute-done | bytes 178208 | tf_op jit(solution)/shard_map/ppermute | solution.py:20
  48.4 3.0 %collective-permute-done.14 = bf16[8,11136]{1,0:T(8,128)(2,1)S(1)} collective-permute-done((bf16[8,11136]{1,0:T(8,128)(2,1)S(1)}, bf16[8,11136]{1,0:T(8,128)(2,1)S(1)}, u32[]{:S(2)}, u32[]{:S(2)}) %collective-permute-start.14) | collective-permute-done | bytes 178208 | tf_op jit(solution)/shard_map/ppermute | solution.py:20
  51.4 0.1 add_convert_fusion
  51.5 0.1 fusion.4
  51.6 2.1 %collective-permute-start.16 = (bf16[2,11136]{1,0:T(2,128)(2,1)S(1)}, bf16[2,11136]{1,0:T(2,128)(2,1)S(1)}, u32[]{:S(2)}, u32[]{:S(2)}) collective-permute-start(bf16[2,11136]{1,0:T(2,128)(2,1)S(1)} %get-tuple-element.34), channel_id=1, source_target_pairs={{0,8},{2,10},{4,12},{6,14},{8,0},{10,2},{12,4},{14,6},{16,24},{18,... | collective-permute-start | bytes 133640 | tf_op jit(solution)/shard_map/ppermute | solution.py:20
  53.7 0.9 %collective-permute-start.17 = (bf16[2,11136]{1,0:T(2,128)(2,1)S(1)}, bf16[2,11136]{1,0:T(2,128)(2,1)S(1)}, u32[]{:S(2)}, u32[]{:S(2)}) collective-permute-start(bf16[2,11136]{1,0:T(2,128)(2,1)S(1)} %get-tuple-element.33), channel_id=1, source_target_pairs={{0,16},{2,18},{4,20},{6,22},{8,24},{10,26},{12,28},{14,30},{16,0},... | collective-permute-start | bytes 133640 | tf_op jit(solution)/shard_map/ppermute | solution.py:20
  54.6 1.5 %collective-permute-start.18 = (bf16[2,11136]{1,0:T(2,128)(2,1)S(1)}, bf16[2,11136]{1,0:T(2,128)(2,1)S(1)}, u32[]{:S(2)}, u32[]{:S(2)}) collective-permute-start(bf16[2,11136]{1,0:T(2,128)(2,1)S(1)} %get-tuple-element.32), channel_id=1, source_target_pairs={{0,24},{2,26},{4,28},{6,30},{8,16},{10,18},{12,20},{14,22},{16,8},... | collective-permute-start | bytes 133640 | tf_op jit(solution)/shard_map/ppermute | solution.py:20
  56.2 3.4 %collective-permute-done.17.refs_2_ = bf16[2,11136]{1,0:T(2,128)(2,1)S(1)} collective-permute-done((bf16[2,11136]{1,0:T(2,128)(2,1)S(1)}, bf16[2,11136]{1,0:T(2,128)(2,1)S(1)}, u32[]{:S(2)}, u32[]{:S(2)}) %collective-permute-start.17) | collective-permute-done | bytes 44576 | tf_op jit(solution)/shard_map/ppermute | solution.py:20
  59.6 1.0 %collective-permute-done.18.refs_3_ = bf16[2,11136]{1,0:T(2,128)(2,1)S(1)} collective-permute-done((bf16[2,11136]{1,0:T(2,128)(2,1)S(1)}, bf16[2,11136]{1,0:T(2,128)(2,1)S(1)}, u32[]{:S(2)}, u32[]{:S(2)}) %collective-permute-start.18) | collective-permute-done | bytes 44576 | tf_op jit(solution)/shard_map/ppermute | solution.py:20
  60.6 0.2 shard_map.163
  60.8 1.6 %collective-permute-start.21 = (bf16[2,5504]{1,0:T(2,128)(2,1)S(1)}, bf16[2,5504]{1,0:T(2,128)(2,1)S(1)}, u32[]{:S(2)}, u32[]{:S(2)}) collective-permute-start(bf16[2,5504]{1,0:T(2,128)(2,1)S(1)} %shard_map.163), channel_id=1, source_target_pairs={{0,24},{2,26},{4,28},{6,30},{8,16},{10,18},{12,20},{14,22},{16,8},... | collective-permute-start | bytes 66056 | tf_op jit(solution)/shard_map/ppermute | solution.py:20
  62.4 0.0 collective-permute-start.20
  62.4 2.8 %collective-permute-start.19 = (bf16[2,5504]{1,0:T(2,128)(2,1)S(1)}, bf16[2,5504]{1,0:T(2,128)(2,1)S(1)}, u32[]{:S(2)}, u32[]{:S(2)}) collective-permute-start(bf16[2,5504]{1,0:T(2,128)(2,1)S(1)} %shard_map.163), channel_id=1, source_target_pairs={{0,8},{2,10},{4,12},{6,14},{8,0},{10,2},{12,4},{14,6},{16,24},{18,... | collective-permute-start | bytes 66056 | tf_op jit(solution)/shard_map/ppermute | solution.py:20
  65.2 1.2 %collective-permute-done.21 = bf16[2,5504]{1,0:T(2,128)(2,1)S(1)} collective-permute-done((bf16[2,5504]{1,0:T(2,128)(2,1)S(1)}, bf16[2,5504]{1,0:T(2,128)(2,1)S(1)}, u32[]{:S(2)}, u32[]{:S(2)}) %collective-permute-start.21) | collective-permute-done | bytes 22048 | tf_op jit(solution)/shard_map/ppermute | solution.py:20
  66.4 0.7 collective-permute-done.20
  67.2 0.1 collective-permute-done.19
  67.2 0.1 pad_maximum_fusion.refs_0_
  67.3 1.3 %collective-permute-start.22 = (bf16[8,5504]{1,0:T(8,128)(2,1)S(1)}, bf16[8,5504]{1,0:T(8,128)(2,1)S(1)}, u32[]{:S(2)}, u32[]{:S(2)}) collective-permute-start(bf16[8,5504]{1,0:T(8,128)(2,1)S(1)} %pad_maximum_fusion.refs_0_), channel_id=1, source_target_pairs={{0,2},{2,0},{4,6},{6,4},{8,10},{10,8},{12,14},{14,12},{16,18},{18,... | collective-permute-start | bytes 264200 | tf_op jit(solution)/shard_map/ppermute | solution.py:20
  68.6 0.6 collective-permute-start.23
  69.2 1.7 %collective-permute-start.24 = (bf16[8,5504]{1,0:T(8,128)(2,1)S(1)}, bf16[8,5504]{1,0:T(8,128)(2,1)S(1)}, u32[]{:S(2)}, u32[]{:S(2)}) collective-permute-start(bf16[8,5504]{1,0:T(8,128)(2,1)S(1)} %pad_maximum_fusion.refs_0_), channel_id=1, source_target_pairs={{0,6},{2,4},{4,2},{6,0},{8,14},{10,12},{12,10},{14,8},{16,22},{18,... | collective-permute-start | bytes 264200 | tf_op jit(solution)/shard_map/ppermute | solution.py:20
  70.9 1.0 %collective-permute-done.22.refs_1_ = bf16[8,5504]{1,0:T(8,128)(2,1)S(1)} collective-permute-done((bf16[8,5504]{1,0:T(8,128)(2,1)S(1)}, bf16[8,5504]{1,0:T(8,128)(2,1)S(1)}, u32[]{:S(2)}, u32[]{:S(2)}) %collective-permute-start.22) | collective-permute-done | bytes 88096 | tf_op jit(solution)/shard_map/ppermute | solution.py:20
  71.9 1.2 %collective-permute-done.23.refs_2_ = bf16[8,5504]{1,0:T(8,128)(2,1)S(1)} collective-permute-done((bf16[8,5504]{1,0:T(8,128)(2,1)S(1)}, bf16[8,5504]{1,0:T(8,128)(2,1)S(1)}, u32[]{:S(2)}, u32[]{:S(2)}) %collective-permute-start.23) | collective-permute-done | bytes 88096 | tf_op jit(solution)/shard_map/ppermute | solution.py:20
  73.1 1.5 %collective-permute-done.24.refs_3_ = bf16[8,5504]{1,0:T(8,128)(2,1)S(1)} collective-permute-done((bf16[8,5504]{1,0:T(8,128)(2,1)S(1)}, bf16[8,5504]{1,0:T(8,128)(2,1)S(1)}, u32[]{:S(2)}, u32[]{:S(2)}) %collective-permute-start.24) | collective-permute-done | bytes 88096 | tf_op jit(solution)/shard_map/ppermute | solution.py:20
  74.6 0.6 shard_map.164.refs_0_
  75.2 0.1 collective-permute-start.25
  75.3 2.2 %shard_map.166 = f32[2,4,256,512]{3,2,1,0:T(8,128)} custom-call(f32[256,24]{1,0:T(8,128)S(1)} %get-tuple-element.30.turned, f32[8,512]{1,0:T(8,128)S(1)} %get-tuple-element.31.values, f32[2,4,256,512]{3,2,1,0:T(8,128)S(1)} %get-tuple-element.19.state), custom_call_target="tpu_custom_call" | custom-call | flops 4194304 | bytes 8388608 | tf_op jit(solution)/shard_map/pallas_call | solution.py:30
  77.5 0.8 shard_map.165
  (19 shorter events, 0.1 us)
Async XLA Ops:
  0.6 17.1 %copy-start.4 = (bf16[512]{0:T(512)(128)(2,1)S(1)}, bf16[512]{0:T(512)(128)(2,1)}, u32[]{:S(2)}) copy-start(bf16[512]{0:T(512)(128)(2,1)} %param.24) | copy-start | bytes 3076
  0.7 22.5 %copy-start.3 = (f32[1024]{0:T(1024)S(1)}, f32[1024]{0:T(1024)}, u32[]{:S(2)}) copy-start(f32[1024]{0:T(1024)} %param.23) | copy-start | bytes 12292
  3.2 7.6 %collective-permute-start.2 = (bf16[8,7296]{1,0:T(8,128)(2,1)S(1)}, bf16[8,7296]{1,0:T(8,128)(2,1)S(1)}, u32[]{:S(2)}, u32[]{:S(2)}) collective-permute-start(bf16[8,7296]{1,0:T(8,128)(2,1)S(1)} %get-tuple-element.23), channel_id=1, source_target_pairs={{0,6},{2,4},{4,2},{6,0},{8,14},{10,12},{12,10},{14,8},{16,22},{18,... | collective-permute-start | bytes 350216 | tf_op jit(solution)/shard_map/ppermute | solution.py:20
  7.2 5.7 %collective-permute-start.1 = (bf16[8,7296]{1,0:T(8,128)(2,1)S(1)}, bf16[8,7296]{1,0:T(8,128)(2,1)S(1)}, u32[]{:S(2)}, u32[]{:S(2)}) collective-permute-start(bf16[8,7296]{1,0:T(8,128)(2,1)S(1)} %get-tuple-element.22), channel_id=1, source_target_pairs={{0,4},{2,6},{4,0},{6,2},{8,12},{10,14},{12,8},{14,10},{16,20},{18,... | collective-permute-start | bytes 350216 | tf_op jit(solution)/shard_map/ppermute | solution.py:20
  7.7 5.4 %collective-permute-start = (bf16[8,7296]{1,0:T(8,128)(2,1)S(1)}, bf16[8,7296]{1,0:T(8,128)(2,1)S(1)}, u32[]{:S(2)}, u32[]{:S(2)}) collective-permute-start(bf16[8,7296]{1,0:T(8,128)(2,1)S(1)} %get-tuple-element.21), channel_id=1, source_target_pairs={{0,2},{2,0},{4,6},{6,4},{8,10},{10,8},{12,14},{14,12},{16,18},{18,... | collective-permute-start | bytes 350216 | tf_op jit(solution)/shard_map/ppermute | solution.py:20
  13.3 7.2 %collective-permute-start.3 = (bf16[2,7296]{1,0:T(2,128)(2,1)S(1)}, bf16[2,7296]{1,0:T(2,128)(2,1)S(1)}, u32[]{:S(2)}, u32[]{:S(2)}) collective-permute-start(bf16[2,7296]{1,0:T(2,128)(2,1)S(1)} %get-tuple-element.38), channel_id=1, source_target_pairs={{0,8},{2,10},{4,12},{6,14},{8,0},{10,2},{12,4},{14,6},{16,24},{18,... | collective-permute-start | bytes 87560 | tf_op jit(solution)/shard_map/ppermute | solution.py:20
  14.9 5.6 %collective-permute-start.4 = (bf16[2,7296]{1,0:T(2,128)(2,1)S(1)}, bf16[2,7296]{1,0:T(2,128)(2,1)S(1)}, u32[]{:S(2)}, u32[]{:S(2)}) collective-permute-start(bf16[2,7296]{1,0:T(2,128)(2,1)S(1)} %get-tuple-element.37), channel_id=1, source_target_pairs={{0,16},{2,18},{4,20},{6,22},{8,24},{10,26},{12,28},{14,30},{16,0},... | collective-permute-start | bytes 87560 | tf_op jit(solution)/shard_map/ppermute | solution.py:20
  17.5 5.7 %collective-permute-start.5 = (bf16[2,7296]{1,0:T(2,128)(2,1)S(1)}, bf16[2,7296]{1,0:T(2,128)(2,1)S(1)}, u32[]{:S(2)}, u32[]{:S(2)}) collective-permute-start(bf16[2,7296]{1,0:T(2,128)(2,1)S(1)} %get-tuple-element.36), channel_id=1, source_target_pairs={{0,24},{2,26},{4,28},{6,30},{8,16},{10,18},{12,20},{14,22},{16,8},... | collective-permute-start | bytes 87560 | tf_op jit(solution)/shard_map/ppermute | solution.py:20
  17.8 20.1 %copy-start.5 = (bf16[256]{0:T(256)(128)(2,1)S(1)}, bf16[256]{0:T(256)(128)(2,1)}, u32[]{:S(2)}) copy-start(bf16[256]{0:T(256)(128)(2,1)} %param.17) | copy-start | bytes 1540
  17.8 21.3 %copy-start = (bf16[256,5504]{1,0:T(8,128)(2,1)S(1)}, bf16[256,5504]{1,0:T(8,128)(2,1)}, u32[]{:S(2)}) copy-start(bf16[256,5504]{1,0:T(8,128)(2,1)} %gate.1) | copy-start | bytes 8454148
  17.8 21.3 %copy-start.1 = (bf16[256,5504]{1,0:T(8,128)(2,1)S(1)}, bf16[256,5504]{1,0:T(8,128)(2,1)}, u32[]{:S(2)}) copy-start(bf16[256,5504]{1,0:T(8,128)(2,1)} %up.1) | copy-start | bytes 8454148
  24.3 5.5 %collective-permute-start.8 = (bf16[2,2048]{1,0:T(2,128)(2,1)S(1)}, bf16[2,2048]{1,0:T(2,128)(2,1)S(1)}, u32[]{:S(2)}, u32[]{:S(2)}) collective-permute-start(bf16[2,2048]{1,0:T(2,128)(2,1)S(1)} %get-tuple-element.24), channel_id=1, source_target_pairs={{0,24},{2,26},{4,28},{6,30},{8,16},{10,18},{12,20},{14,22},{16,8},... | collective-permute-start | bytes 24584 | tf_op jit(solution)/shard_map/ppermute | solution.py:20
  25.3 4.7 %collective-permute-start.7 = (bf16[2,2048]{1,0:T(2,128)(2,1)S(1)}, bf16[2,2048]{1,0:T(2,128)(2,1)S(1)}, u32[]{:S(2)}, u32[]{:S(2)}) collective-permute-start(bf16[2,2048]{1,0:T(2,128)(2,1)S(1)} %get-tuple-element.24), channel_id=1, source_target_pairs={{0,16},{2,18},{4,20},{6,22},{8,24},{10,26},{12,28},{14,30},{16,0},... | collective-permute-start | bytes 24584 | tf_op jit(solution)/shard_map/ppermute | solution.py:20
  25.3 5.1 %collective-permute-start.6 = (bf16[2,2048]{1,0:T(2,128)(2,1)S(1)}, bf16[2,2048]{1,0:T(2,128)(2,1)S(1)}, u32[]{:S(2)}, u32[]{:S(2)}) collective-permute-start(bf16[2,2048]{1,0:T(2,128)(2,1)S(1)} %get-tuple-element.24), channel_id=1, source_target_pairs={{0,8},{2,10},{4,12},{6,14},{8,0},{10,2},{12,4},{14,6},{16,24},{18,... | collective-permute-start | bytes 24584 | tf_op jit(solution)/shard_map/ppermute | solution.py:20
  30.5 4.0 %collective-permute-start.9 = (bf16[8,2048]{1,0:T(8,128)(2,1)S(1)}, bf16[8,2048]{1,0:T(8,128)(2,1)S(1)}, u32[]{:S(2)}, u32[]{:S(2)}) collective-permute-start(bf16[8,2048]{1,0:T(8,128)(2,1)S(1)} %pad_maximum_fusion.1.refs_0_), channel_id=1, source_target_pairs={{0,2},{2,0},{4,6},{6,4},{8,10},{10,8},{12,14},{14,12},{16,18},{18,... | collective-permute-start | bytes 98312 | tf_op jit(solution)/shard_map/ppermute | solution.py:20
  32.1 3.9 %collective-permute-start.10 = (bf16[8,2048]{1,0:T(8,128)(2,1)S(1)}, bf16[8,2048]{1,0:T(8,128)(2,1)S(1)}, u32[]{:S(2)}, u32[]{:S(2)}) collective-permute-start(bf16[8,2048]{1,0:T(8,128)(2,1)S(1)} %pad_maximum_fusion.1.refs_0_), channel_id=1, source_target_pairs={{0,4},{2,6},{4,0},{6,2},{8,12},{10,14},{12,8},{14,10},{16,20},{18,... | collective-permute-start | bytes 98312 | tf_op jit(solution)/shard_map/ppermute | solution.py:20
  32.8 4.8 %collective-permute-start.11 = (bf16[8,2048]{1,0:T(8,128)(2,1)S(1)}, bf16[8,2048]{1,0:T(8,128)(2,1)S(1)}, u32[]{:S(2)}, u32[]{:S(2)}) collective-permute-start(bf16[8,2048]{1,0:T(8,128)(2,1)S(1)} %pad_maximum_fusion.1.refs_0_), channel_id=1, source_target_pairs={{0,6},{2,4},{4,2},{6,0},{8,14},{10,12},{12,10},{14,8},{16,22},{18,... | collective-permute-start | bytes 98312 | tf_op jit(solution)/shard_map/ppermute | solution.py:20
  37.6 37.0 %copy-start.2 = (bf16[5504,256]{1,0:T(8,128)(2,1)S(1)}, bf16[5504,256]{1,0:T(8,128)(2,1)}, u32[]{:S(2)}) copy-start(bf16[5504,256]{1,0:T(8,128)(2,1)} %weight.3) | copy-start | bytes 8454148
  37.9 1.2 %collective-permute-start.12 = (bf16[32,256]{1,0:T(8,128)(2,1)S(1)}, bf16[32,256]{1,0:T(8,128)(2,1)S(1)}, u32[]{:S(2)}, u32[]{:S(2)}) collective-permute-start(bf16[32,256]{1,0:T(8,128)(2,1)S(1)} %shard_map.161.refs_0_), channel_id=1, source_target_pairs={{0,1},{1,0},{2,3},{3,2},{4,5},{5,4},{6,7},{7,6},{8,9},{9,8},{10,11... | collective-permute-start | bytes 49160 | tf_op jit(solution)/shard_map/ppermute | solution.py:20
  40.0 8.4 %collective-permute-start.15 = (bf16[8,11136]{1,0:T(8,128)(2,1)S(1)}, bf16[8,11136]{1,0:T(8,128)(2,1)S(1)}, u32[]{:S(2)}, u32[]{:S(2)}) collective-permute-start(bf16[8,11136]{1,0:T(8,128)(2,1)S(1)} %get-tuple-element.29), channel_id=1, source_target_pairs={{0,6},{2,4},{4,2},{6,0},{8,14},{10,12},{12,10},{14,8},{16,22},{18,... | collective-permute-start | bytes 534536 | tf_op jit(solution)/shard_map/ppermute | solution.py:20
  41.3 10.1 %collective-permute-start.14 = (bf16[8,11136]{1,0:T(8,128)(2,1)S(1)}, bf16[8,11136]{1,0:T(8,128)(2,1)S(1)}, u32[]{:S(2)}, u32[]{:S(2)}) collective-permute-start(bf16[8,11136]{1,0:T(8,128)(2,1)S(1)} %get-tuple-element.28), channel_id=1, source_target_pairs={{0,4},{2,6},{4,0},{6,2},{8,12},{10,14},{12,8},{14,10},{16,20},{18,... | collective-permute-start | bytes 534536 | tf_op jit(solution)/shard_map/ppermute | solution.py:20
  42.8 8.6 %collective-permute-start.13 = (bf16[8,11136]{1,0:T(8,128)(2,1)S(1)}, bf16[8,11136]{1,0:T(8,128)(2,1)S(1)}, u32[]{:S(2)}, u32[]{:S(2)}) collective-permute-start(bf16[8,11136]{1,0:T(8,128)(2,1)S(1)} %get-tuple-element.27), channel_id=1, source_target_pairs={{0,2},{2,0},{4,6},{6,4},{8,10},{10,8},{12,14},{14,12},{16,18},{18,... | collective-permute-start | bytes 534536 | tf_op jit(solution)/shard_map/ppermute | solution.py:20
  51.6 4.5 %collective-permute-start.16 = (bf16[2,11136]{1,0:T(2,128)(2,1)S(1)}, bf16[2,11136]{1,0:T(2,128)(2,1)S(1)}, u32[]{:S(2)}, u32[]{:S(2)}) collective-permute-start(bf16[2,11136]{1,0:T(2,128)(2,1)S(1)} %get-tuple-element.34), channel_id=1, source_target_pairs={{0,8},{2,10},{4,12},{6,14},{8,0},{10,2},{12,4},{14,6},{16,24},{18,... | collective-permute-start | bytes 133640 | tf_op jit(solution)/shard_map/ppermute | solution.py:20
  53.7 5.9 %collective-permute-start.17 = (bf16[2,11136]{1,0:T(2,128)(2,1)S(1)}, bf16[2,11136]{1,0:T(2,128)(2,1)S(1)}, u32[]{:S(2)}, u32[]{:S(2)}) collective-permute-start(bf16[2,11136]{1,0:T(2,128)(2,1)S(1)} %get-tuple-element.33), channel_id=1, source_target_pairs={{0,16},{2,18},{4,20},{6,22},{8,24},{10,26},{12,28},{14,30},{16,0},... | collective-permute-start | bytes 133640 | tf_op jit(solution)/shard_map/ppermute | solution.py:20
  54.6 5.9 %collective-permute-start.18 = (bf16[2,11136]{1,0:T(2,128)(2,1)S(1)}, bf16[2,11136]{1,0:T(2,128)(2,1)S(1)}, u32[]{:S(2)}, u32[]{:S(2)}) collective-permute-start(bf16[2,11136]{1,0:T(2,128)(2,1)S(1)} %get-tuple-element.32), channel_id=1, source_target_pairs={{0,24},{2,26},{4,28},{6,30},{8,16},{10,18},{12,20},{14,22},{16,8},... | collective-permute-start | bytes 133640 | tf_op jit(solution)/shard_map/ppermute | solution.py:20
  60.8 5.7 %collective-permute-start.21 = (bf16[2,5504]{1,0:T(2,128)(2,1)S(1)}, bf16[2,5504]{1,0:T(2,128)(2,1)S(1)}, u32[]{:S(2)}, u32[]{:S(2)}) collective-permute-start(bf16[2,5504]{1,0:T(2,128)(2,1)S(1)} %shard_map.163), channel_id=1, source_target_pairs={{0,24},{2,26},{4,28},{6,30},{8,16},{10,18},{12,20},{14,22},{16,8},... | collective-permute-start | bytes 66056 | tf_op jit(solution)/shard_map/ppermute | solution.py:20
  62.4 4.8 %collective-permute-start.20 = (bf16[2,5504]{1,0:T(2,128)(2,1)S(1)}, bf16[2,5504]{1,0:T(2,128)(2,1)S(1)}, u32[]{:S(2)}, u32[]{:S(2)}) collective-permute-start(bf16[2,5504]{1,0:T(2,128)(2,1)S(1)} %shard_map.163), channel_id=1, source_target_pairs={{0,16},{2,18},{4,20},{6,22},{8,24},{10,26},{12,28},{14,30},{16,0},... | collective-permute-start | bytes 66056 | tf_op jit(solution)/shard_map/ppermute | solution.py:20
  62.4 4.8 %collective-permute-start.19 = (bf16[2,5504]{1,0:T(2,128)(2,1)S(1)}, bf16[2,5504]{1,0:T(2,128)(2,1)S(1)}, u32[]{:S(2)}, u32[]{:S(2)}) collective-permute-start(bf16[2,5504]{1,0:T(2,128)(2,1)S(1)} %shard_map.163), channel_id=1, source_target_pairs={{0,8},{2,10},{4,12},{6,14},{8,0},{10,2},{12,4},{14,6},{16,24},{18,... | collective-permute-start | bytes 66056 | tf_op jit(solution)/shard_map/ppermute | solution.py:20
  67.3 4.6 %collective-permute-start.22 = (bf16[8,5504]{1,0:T(8,128)(2,1)S(1)}, bf16[8,5504]{1,0:T(8,128)(2,1)S(1)}, u32[]{:S(2)}, u32[]{:S(2)}) collective-permute-start(bf16[8,5504]{1,0:T(8,128)(2,1)S(1)} %pad_maximum_fusion.refs_0_), channel_id=1, source_target_pairs={{0,2},{2,0},{4,6},{6,4},{8,10},{10,8},{12,14},{14,12},{16,18},{18,... | collective-permute-start | bytes 264200 | tf_op jit(solution)/shard_map/ppermute | solution.py:20
  68.6 4.5 %collective-permute-start.23 = (bf16[8,5504]{1,0:T(8,128)(2,1)S(1)}, bf16[8,5504]{1,0:T(8,128)(2,1)S(1)}, u32[]{:S(2)}, u32[]{:S(2)}) collective-permute-start(bf16[8,5504]{1,0:T(8,128)(2,1)S(1)} %pad_maximum_fusion.refs_0_), channel_id=1, source_target_pairs={{0,4},{2,6},{4,0},{6,2},{8,12},{10,14},{12,8},{14,10},{16,20},{18,... | collective-permute-start | bytes 264200 | tf_op jit(solution)/shard_map/ppermute | solution.py:20
  69.2 5.4 %collective-permute-start.24 = (bf16[8,5504]{1,0:T(8,128)(2,1)S(1)}, bf16[8,5504]{1,0:T(8,128)(2,1)S(1)}, u32[]{:S(2)}, u32[]{:S(2)}) collective-permute-start(bf16[8,5504]{1,0:T(8,128)(2,1)S(1)} %pad_maximum_fusion.refs_0_), channel_id=1, source_target_pairs={{0,6},{2,4},{4,2},{6,0},{8,14},{10,12},{12,10},{14,8},{16,22},{18,... | collective-permute-start | bytes 264200 | tf_op jit(solution)/shard_map/ppermute | solution.py:20
  75.2 2.3 %collective-permute-start.25 = (bf16[32,256]{1,0:T(8,128)(2,1)S(1)}, bf16[32,256]{1,0:T(8,128)(2,1)S(1)}, u32[]{:S(2)}, u32[]{:S(2)}) collective-permute-start(bf16[32,256]{1,0:T(8,128)(2,1)S(1)} %shard_map.164.refs_0_), channel_id=1, source_target_pairs={{0,1},{1,0},{2,3},{3,2},{4,5},{5,4},{6,7},{7,6},{8,9},{9,8},{10,11... | collective-permute-start | bytes 49160 | tf_op jit(solution)/shard_map/ppermute | solution.py:20
